TPU v7x, 256 devices: a whole 4x4x8 slice. The times are simulated.
256 devices in a mesh: sp: 16 (over y, x), tp: 16 (over z, core).
Axes of the slice: x: 4, y: 4, z: 8, core: 2. Of those that a mesh axis runs over, the one named last changes fastest.
Arguments:
- gate_b: bfloat16 [8192, 1024], P('sp', 'tp'), may hold values from -6 to 6
- gate_c: bfloat16 [8192, 1024], P('sp', 'tp'), may hold values from -6 to 6
- values_in: bfloat16 [8192, 1024], P('sp', 'tp'), may hold values from -6 to 6
- conv_w: bfloat16 [3, 1024], P(None, 'tp'), may hold values from -3.5 to 3.5
- documents: int32 [8192], P('sp'), may hold values from 0 to 8, never falling along the last dimension, each value on 1 to 4096 neighbouring positions
- w_out: bfloat16 [1024, 2048], replicated, may hold values from -0.1875 to 0.1875
- resid: bfloat16 [8192, 2048], P(('sp', 'tp')), may hold values from -6 to 6
- norm_gain: bfloat16 [2048], replicated, may hold values from 0.099609375 to 1.8984375
- route_ids: int32 [8192, 2], P(('sp', 'tp')), may hold values from 0 to 15, all different within a row; in each aligned block of 32 rows (0 to 31, 32 to 63, ...) at most 8 rows name the same one
- route_weight: float32 [8192, 2], P(('sp', 'tp')), may hold values from 0.2 to 1
- w_gate: bfloat16 [16, 2048, 7168], P('sp', None, 'tp'), may hold values from -0.125 to 0.125
- w_up: bfloat16 [16, 2048, 7168], P('sp', None, 'tp'), may hold values from -0.125 to 0.125
- w_down: bfloat16 [16, 7168, 2048], P('sp', 'tp'), may hold values from -0.0625 to 0.0625
Outputs:
- layer_out: bfloat16 [8192, 2048], P(('sp', 'tp'))
Inputs may be any that keep to these rules, and one draw needn't show every extreme that they name: `route_ids`: each token names two different experts; in the rows of one device no expert is named by more than 8 rows, a bound that some block reaches. `documents`: document numbers never fall along the positions; a document has at most 8192 // 2 positions.
All inputs are finite; a program needn't handle non-finite values.
Results may differ from a plain program's by a relative error of at most 0.018.
Values may be sent and summed in bfloat16 or wider, within the bound.
No kernel may reach another device: no remote copies, remote signals or barrier semaphores. Data moves between devices by JAX's collectives and lax.ppermute only.
A program may use at most 128 MiB of HBM per device.

v0:
```python
import jax
import jax.numpy as jnp
from jax import lax
from jax.sharding import PartitionSpec as P


def passed_along(block, axis, distance):
    devices = range(lax.axis_size(axis))
    route = [(i - distance, i) for i in devices if i - distance in devices]
    return lax.ppermute(block, axis, route)


def local(
    gate_b,
    gate_c,
    values_in,
    conv_w,
    documents,
    w_out,
    resid,
    norm_gain,
    route_ids,
    route_weight,
    w_gate,
    w_up,
    w_down,
):
    seq_rows = gate_b.shape[0]
    local_rows = resid.shape[0]
    model_width = resid.shape[1]
    last_rows = jnp.stack([gate_c[seq_rows - 2 :], values_in[seq_rows - 2 :]])
    before, before_docs = passed_along((last_rows, documents[seq_rows - 2 :]), "sp", 1)
    products = jnp.concatenate(
        [
            before[0].astype(jnp.float32) * before[1].astype(jnp.float32),
            gate_c.astype(jnp.float32) * values_in.astype(jnp.float32),
        ],
        axis=0,
    )
    docs_all = jnp.concatenate([before_docs, documents], axis=0)
    kernel_taps = conv_w.astype(jnp.float32)
    near_mask = (docs_all[1:-1] == documents).astype(jnp.float32)[:, None]
    far_mask = (docs_all[:-2] == documents).astype(jnp.float32)[:, None]
    convolved = (
        kernel_taps[2] * products[2:]
        + kernel_taps[1] * products[1:-1] * near_mask
        + kernel_taps[0] * products[:-2] * far_mask
    )
    mixed_rows = (gate_b.astype(jnp.float32) * convolved).astype(jnp.bfloat16)
    token_rows = lax.all_to_all(mixed_rows, "tp", split_axis=0, concat_axis=1, tiled=True)
    projected = jnp.dot(token_rows, w_out, preferred_element_type=jnp.float32)
    hidden_state = (resid.astype(jnp.float32) + projected).astype(jnp.bfloat16)
    state_wide = hidden_state.astype(jnp.float32)
    normed = (
        state_wide
        * lax.rsqrt(jnp.mean(state_wide * state_wide, axis=-1, keepdims=True) + 1e-06)
        * norm_gain.astype(jnp.float32)
    ).astype(jnp.bfloat16)
    experts = lax.axis_size("sp") * w_gate.shape[0]
    capacity = 4 * local_rows // experts
    flat_ids = route_ids.reshape(-1)
    one_hot = (flat_ids[:, None] == jnp.arange(experts, dtype=jnp.int32)[None, :]).astype(jnp.int32)
    rank_in = jnp.sum((jnp.cumsum(one_hot, axis=0) - one_hot) * one_hot, axis=1)
    slot_index = flat_ids * capacity + rank_in
    placement = (
        slot_index[:, None] == jnp.arange(experts * capacity, dtype=jnp.int32)[None, :]
    ).astype(jnp.bfloat16)
    repeated = jnp.repeat(normed, 2, axis=0)
    dispatch = jnp.einsum(
        "js,jd->sd", placement, repeated, preferred_element_type=jnp.float32
    ).astype(jnp.bfloat16)
    dispatch = dispatch.reshape(experts, capacity, model_width)
    gathered_piece = lax.all_gather(
        lax.all_to_all(dispatch, "sp", split_axis=0, concat_axis=0, tiled=True),
        "tp",
        axis=0,
        tiled=True,
    )
    flat_rows = gathered_piece.reshape(-1, model_width)
    gate_part = jnp.dot(flat_rows, w_gate[0], preferred_element_type=jnp.float32)
    up_part = jnp.dot(flat_rows, w_up[0], preferred_element_type=jnp.float32)
    activated = (jax.nn.silu(gate_part) * up_part).astype(jnp.bfloat16)
    partial_value = jnp.dot(activated, w_down[0], preferred_element_type=jnp.float32)
    partial_value = partial_value.reshape(
        gathered_piece.shape[0], gathered_piece.shape[1], model_width
    )
    summed = lax.psum_scatter(
        partial_value.astype(jnp.bfloat16), "tp", scatter_dimension=0, tiled=True
    )
    returned = lax.all_to_all(summed, "sp", split_axis=0, concat_axis=0, tiled=True)
    picked = jnp.take(
        returned.reshape(experts * capacity, model_width), slot_index, axis=0
    ).reshape(local_rows, 2, model_width)
    combined = jnp.sum(route_weight[:, :, None] * picked.astype(jnp.float32), axis=1)
    return (hidden_state.astype(jnp.float32) + combined).astype(jnp.bfloat16)


def solution(mesh):
    return jax.shard_map(
        local,
        mesh=mesh,
        in_specs=(
            P("sp", "tp"),
            P("sp", "tp"),
            P("sp", "tp"),
            P(None, "tp"),
            P("sp"),
            P(),
            P(("sp", "tp"), None),
            P(),
            P(("sp", "tp"), None),
            P(("sp", "tp"), None),
            P("sp", None, "tp"),
            P("sp", None, "tp"),
            P("sp", "tp", None),
        ),
        out_specs=P(("sp", "tp"), None),
        check_vma=False,
    )
```

profile of v0, /device:TPU:2, one launch (start us, length us, event | category | flops | bytes accessed | tf_op | source)
XLA Modules:
  0.0 234.4 jit_solution(8225996941570353827)
XLA Ops:
  6.5 0.0 copy-start
  6.5 0.9 slice.43
  7.4 3.4 %collective-permute-start.1 = (s32[2]{0:T(128)S(1)}, s32[2]{0:T(128)S(1)}, u32[]{:S(2)}, u32[]{:S(2)}) collective-permute-start(s32[2]{0:T(128)S(1)} %slice.43), channel_id=1, source_target_pairs={{0,16},{16,32},{32,48},{48,64},{64,80},{80,96},{96,112},{112,128},... | collective-permute-start | bytes 32 | tf_op jit(solution)/shard_map/ppermute | solution.py:10
  10.8 0.8 slice.38
  11.6 0.1 copy.45
  11.7 0.8 slice.39
  12.5 0.1 copy.46
  12.6 3.1 %collective-permute-start = (bf16[2,2,64]{2,1,0:T(2,128)(2,1)S(1)}, bf16[2,2,64]{2,1,0:T(2,128)(2,1)S(1)}, u32[]{:S(2)}, u32[]{:S(2)}) collective-permute-start(bf16[2,2,64]{2,1,0:T(2,128)(2,1)S(1)} %pad_maximum_fusion.1), channel_id=1, source_target_pairs={{0,16},{16,32},{32,48},{48,64},{64,80},{80,96},{96,112},{112,128},... | collective-permute-start | bytes 1544 | tf_op jit(solution)/shard_map/ppermute | solution.py:10
  15.7 0.9 convert_multiply_fusion
  16.6 0.7 convert_element_type.66
  17.3 0.7 convert_element_type.77
  18.0 0.8 copy.51
  18.8 0.1 reshape.83
  18.9 0.1 fusion.22
  18.9 0.1 reduce_window_sum.11
  19.0 0.2 select_reduce_fusion
  19.2 0.0 collective-permute-done.1
  19.2 0.8 pad_add_fusion
  20.0 0.8 fusion.24
  20.7 0.0 collective-permute-done
  20.8 0.1 copy.47
  20.9 1.0 fusion.19
  21.9 0.1 copy.48
  22.0 0.8 reshape.97
  22.8 8.6 %all-to-all-start = ((bf16[16,2,1024]{2,1,0:T(2,128)(2,1)}), bf16[16,2,1024]{2,1,0:T(2,128)(2,1)S(1)}, u32[]{:S(2)}, u32[]{:S(2)}) async-start(bf16[16,2,1024]{2,1,0:T(2,128)(2,1)} %reshape.97), calls=%async_computation | async-start | bytes 131072 | tf_op jit(solution)/shard_map/all_to_all | solution.py:50
  31.3 0.0 all-gather.2.cloned.1.call-start
  31.4 7.7 %all-to-all-done = bf16[16,2,1024]{2,1,0:T(2,128)(2,1)S(1)} async-done(((bf16[16,2,1024]{2,1,0:T(2,128)(2,1)}), bf16[16,2,1024]{2,1,0:T(2,128)(2,1)S(1)}, u32[]{:S(2)}, u32[]{:S(2)}) %all-to-all-start) | async-done | bytes 65568 | tf_op jit(solution)/shard_map/all_to_all | solution.py:50
  39.1 0.1 reshape.98
  39.3 0.1 copy.49
  39.3 0.1 all_to_all.23
  39.5 3.1 %multiply_reduce_fusion.1 = (f32[32]{0:T(128)S(1)}, f32[32,2048]{1,0:T(8,128)S(1)}) fusion(bf16[32,1024]{1,0:T(8,128)(2,1)S(1)} %all_to_all.23, bf16[1024,2048]{1,0:T(8,128)(2,1)} %param.18, bf16[32,2048]{1,0:T(8,128)(2,1)} %param.19), kind=kOutput, calls=%fused_computation.20 | convolution fusion | flops 134610912 | bytes 4653184 | tf_op jit(solution)/shard_map/dot_general | solution.py:51
  42.6 0.1 multiply_convert_fusion.1
  42.7 0.1 broadcast_in_dim.10
  42.9 0.1 reshape.84
  43.0 0.4 fusion.6
  43.4 17.8 %all_to_all.29 = bf16[16,8,2048]{2,1,0:T(8,128)(2,1)} all-to-all(bf16[16,8,2048]{2,1,0:T(8,128)(2,1)S(1)} %fusion.6), channel_id=1, replica_groups=mesh['sp'=16,'tp'=16] {'sp'}, dimensions={0} | all-to-all | bytes 1048576 | tf_op jit(solution)/shard_map/all_to_all | solution.py:74
  61.3 0.0 all-gather.2.cloned.1.call-update
  61.3 0.0 reduce-scatter.2.cloned.1.call-start
  61.3 49.6 %all-gather.2.cloned.1.call-done = bf16[256,8,2048]{2,1,0:T(8,128)(2,1)} async-done(((bf16[16,8,2048]{2,1,0:T(8,128)(2,1)}), bf16[256,8,2048]{2,1,0:T(8,128)(2,1)}) %all-gather.2.cloned.1.call-update) | async-done | bytes 8388624 | tf_op jit(solution)/shard_map/all_gather | solution.py:73
  110.9 0.0 copy-start.3
  111.0 7.2 %fusion.2 = f32[2048,448]{0,1:T(8,128)S(1)} fusion(bf16[256,8,2048]{2,1,0:T(8,128)(2,1)} %all-gather.2.cloned.1.call-done, bf16[1,2048,448]{1,2,0:T(8,128)(2,1)} %param.23), kind=kOutput, calls=%fused_computation.3 | convolution fusion | flops 3758096384 | bytes 13893632 | tf_op jit(solution)/shard_map/dot_general | solution.py:80
  118.2 0.0 copy-done.3
  118.2 0.0 copy-done.4
  118.2 5.5 %multiply_convert_fusion = bf16[2048,448]{0,1:T(8,128)(2,1)} fusion(f32[2048,448]{0,1:T(8,128)S(1)} %fusion.2, bf16[256,8,2048]{2,1,0:T(8,128)(2,1)S(1)} %copy-done.3, bf16[1,2048,448]{1,2,0:T(8,128)(2,1)S(1)} %copy-done.4), kind=kOutput, calls=%fused_computation.6 | convolution fusion | flops 3763601408 | bytes 15728640 | tf_op jit(solution)/shard_map/dot_general | solution.py:81
  123.7 3.8 %copy.54 = bf16[2048,448]{1,0:T(8,128)(2,1)} copy(bf16[2048,448]{0,1:T(8,128)(2,1)} %multiply_convert_fusion) | data formatting | bytes 3670016 | tf_op jit(solution)/shard_map/convert_element_type | solution.py:82
  127.5 0.0 copy-done
  127.5 9.2 %convolution_convert_fusion = bf16[256,8,2048]{2,0,1:T(8,128)(2,1)} fusion(bf16[256,8,448]{2,1,0:T(8,128)(2,1)} %bitcast.43, bf16[1,448,2048]{2,1,0:T(8,128)(2,1)S(1)} %copy-done), kind=kOutput, calls=%fused_computation.5 | convolution fusion | flops 3762290688 | bytes 12058624 | tf_op jit(solution)/shard_map/dot_general | solution.py:83
  136.7 0.0 reduce-scatter.2.cloned.1.call-update
  136.7 0.1 reduce_sum.32
  136.8 0.5 copy-done.1
  137.4 0.1 copy.57
  137.4 0.1 mul.151
  137.6 0.1 copy.52
  137.6 68.4 %reduce-scatter.2.cloned.1.call-done = bf16[16,8,2048]{2,0,1:T(8,128)(2,1)} async-done(((bf16[256,8,2048]{2,0,1:T(8,128)(2,1)}), bf16[16,8,2048]{2,0,1:T(8,128)(2,1)}) %reduce-scatter.2.cloned.1.call-update) | async-done | bytes 524304 | tf_op jit(solution)/shard_map/reduce_scatter | solution.py:87
  206.1 2.1 copy.56
  208.2 7.3 %all-to-all-start.2 = ((bf16[16,8,2048]{2,1,0:T(8,128)(2,1)}), bf16[16,8,2048]{2,1,0:T(8,128)(2,1)S(1)}, u32[]{:S(2)}, u32[]{:S(2)}) async-start(bf16[16,8,2048]{2,1,0:T(8,128)(2,1)} %copy.56), calls=%async_computation.3 | async-start | bytes 1048576 | tf_op jit(solution)/shard_map/all_to_all | solution.py:90
  215.5 0.1 copy.53
  215.6 0.0 copy-done.2
  215.6 0.1 copy.50
  215.7 8.6 %all-to-all-done.2 = bf16[16,8,2048]{2,1,0:T(8,128)(2,1)S(1)} async-done(((bf16[16,8,2048]{2,1,0:T(8,128)(2,1)}), bf16[16,8,2048]{2,1,0:T(8,128)(2,1)S(1)}, u32[]{:S(2)}, u32[]{:S(2)}) %all-to-all-start.2) | async-done | bytes 524320 | tf_op jit(solution)/shard_map/all_to_all | solution.py:90
  224.3 0.7 gather_fusion
  225.0 0.2 gather.7
  225.2 1.7 multiply_reduce_fusion
  226.9 0.7 add_convert_fusion
  (12 shorter events, 0.1 us)
Async XLA Ops:
  6.5 120.9 %copy-start = (bf16[1,448,2048]{2,1,0:T(8,128)(2,1)S(1)}, bf16[1,448,2048]{2,1,0:T(8,128)(2,1)}, u32[]{:S(2)}) copy-start(bf16[1,448,2048]{2,1,0:T(8,128)(2,1)} %param.25) | copy-start | bytes 5505028
  7.4 11.8 %collective-permute-start.1 = (s32[2]{0:T(128)S(1)}, s32[2]{0:T(128)S(1)}, u32[]{:S(2)}, u32[]{:S(2)}) collective-permute-start(s32[2]{0:T(128)S(1)} %slice.43), channel_id=1, source_target_pairs={{0,16},{16,32},{32,48},{48,64},{64,80},{80,96},{96,112},{112,128},... | collective-permute-start | bytes 32 | tf_op jit(solution)/shard_map/ppermute | solution.py:10
  12.6 8.1 %collective-permute-start = (bf16[2,2,64]{2,1,0:T(2,128)(2,1)S(1)}, bf16[2,2,64]{2,1,0:T(2,128)(2,1)S(1)}, u32[]{:S(2)}, u32[]{:S(2)}) collective-permute-start(bf16[2,2,64]{2,1,0:T(2,128)(2,1)S(1)} %pad_maximum_fusion.1), channel_id=1, source_target_pairs={{0,16},{16,32},{32,48},{48,64},{64,80},{80,96},{96,112},{112,128},... | collective-permute-start | bytes 1544 | tf_op jit(solution)/shard_map/ppermute | solution.py:10
  22.8 16.4 %all-to-all-start = ((bf16[16,2,1024]{2,1,0:T(2,128)(2,1)}), bf16[16,2,1024]{2,1,0:T(2,128)(2,1)S(1)}, u32[]{:S(2)}, u32[]{:S(2)}) async-start(bf16[16,2,1024]{2,1,0:T(2,128)(2,1)} %reshape.97), calls=%async_computation | async-start | bytes 131072 | tf_op jit(solution)/shard_map/all_to_all | solution.py:50
  31.3 79.6 %all-gather.2.cloned.1.call-start = ((), (), s32[]{:S(2)}) async-start(), calls=%async_computation.4 | async-start | bytes 8912896 | tf_op jit(solution)/shard_map/all_gather | solution.py:73
  61.3 144.8 %reduce-scatter.2.cloned.1.call-start = ((), (), s32[]{:S(2)}) async-start(), calls=%async_computation.5 | async-start | bytes 8912896 | tf_op jit(solution)/shard_map/reduce_scatter | solution.py:87
  110.9 7.2 %copy-start.3 = (bf16[256,8,2048]{2,1,0:T(8,128)(2,1)S(1)}, bf16[256,8,2048]{2,1,0:T(8,128)(2,1)}, u32[]{:S(2)}) copy-start(bf16[256,8,2048]{2,1,0:T(8,128)(2,1)} %all-gather.2.cloned.1.call-done) | copy-start | bytes 25165828
  111.0 7.2 %copy-start.4 = (bf16[1,2048,448]{1,2,0:T(8,128)(2,1)S(1)}, bf16[1,2048,448]{1,2,0:T(8,128)(2,1)}, u32[]{:S(2)}) copy-start(bf16[1,2048,448]{1,2,0:T(8,128)(2,1)} %param.24) | copy-start | bytes 5505028
  136.7 0.7 copy-start.1
  136.7 78.9 %copy-start.2 = (f32[32,2]{0,1:T(2,128)S(1)}, f32[32,2]{0,1:T(2,128)}, u32[]{:S(2)}) copy-start(f32[32,2]{0,1:T(2,128)} %param.22) | copy-start | bytes 772
  208.2 16.1 %all-to-all-start.2 = ((bf16[16,8,2048]{2,1,0:T(8,128)(2,1)}), bf16[16,8,2048]{2,1,0:T(8,128)(2,1)S(1)}, u32[]{:S(2)}, u32[]{:S(2)}) async-start(bf16[16,8,2048]{2,1,0:T(8,128)(2,1)} %copy.56), calls=%async_computation.3 | async-start | bytes 1048576 | tf_op jit(solution)/shard_map/all_to_all | solution.py:90
Sparse Core Ops, SparseCore 0:
  61.4 49.4 all-gather.1
  136.8 69.2 reduce-scatter.1
where the time goes:
time: 235 us; the launch traced here: 234 us
  waiting for transfers between devices  134 us (57%)
  matrix products  25.4 us (11%)
  starting transfers between devices  22.4 us (10%)
  blocking collectives  17.8 us (8%)
  between operations  13.6 us (6%)
  local copies, waits for them, and re-layouts  13.1 us (6%)
  other arithmetic  7.69 us (3%)
    reduce_scatter x1, waiting for transfers between devices, local(): lax.psum_scatter(partial_value.astype(jnp.bfloat16), 'tp', scatter_dimens...  68.4 us
    all_gather x1, waiting for transfers between devices, local(): lax.all_gather(lax.all_to_all(dispatch, 'sp', split_axis=0, concat_axis=0...  49.6 us
    all_to_all x1, blocking collectives, local(): lax.all_to_all(dispatch, 'sp', split_axis=0, concat_axis=0, tiled=True)  17.8 us
    dot_general x1, matrix products, local(): jnp.dot(activated, w_down[0], preferred_element_type=jnp.float32)  9.19 us
    all_to_all x1, starting transfers between devices, local(): lax.all_to_all(mixed_rows, 'tp', split_axis=0, concat_axis=1, tiled=True)  8.57 us
    all_to_all x1, waiting for transfers between devices, local(): lax.all_to_all(summed, 'sp', split_axis=0, concat_axis=0, tiled=True)  8.56 us
    all_to_all x1, waiting for transfers between devices, local(): lax.all_to_all(mixed_rows, 'tp', split_axis=0, concat_axis=1, tiled=True)  7.73 us
    all_to_all x1, starting transfers between devices, local(): lax.all_to_all(summed, 'sp', split_axis=0, concat_axis=0, tiled=True)  7.27 us
  transfers between devices with their start and end apart: 6, of which 4 were waited for; matrix products, arithmetic and copies ran while one was open for 3% of the time, Pallas kernels for 0%

commit v1 on v0

--- a/solution.py
+++ b/solution.py
@@ -70,12 +70,9 @@
         "js,jd->sd", placement, repeated, preferred_element_type=jnp.float32
     ).astype(jnp.bfloat16)
     dispatch = dispatch.reshape(experts, capacity, model_width)
-    gathered_piece = lax.all_gather(
-        lax.all_to_all(dispatch, "sp", split_axis=0, concat_axis=0, tiled=True),
-        "tp",
-        axis=0,
-        tiled=True,
-    )
+    array = lax.all_to_all(dispatch, "sp", split_axis=0, concat_axis=0, tiled=True)
+    copies = jnp.concatenate([array] * lax.axis_size("tp"), axis=0)
+    gathered_piece = lax.all_to_all(copies, "tp", 0, 0, tiled=True)
     flat_rows = gathered_piece.reshape(-1, model_width)
     gate_part = jnp.dot(flat_rows, w_gate[0], preferred_element_type=jnp.float32)
     up_part = jnp.dot(flat_rows, w_up[0], preferred_element_type=jnp.float32)

time: 235 us -> 367 us (1.56)
  blocking collectives: 17.8 us -> 205 us
  waiting for transfers between devices: 134 us -> 81.9 us
    all_to_all x0 -> x1, blocking collectives: none -> 187 us  [local(): gathered_piece = lax.all_to_all(copies, 'tp', 0, 0, tiled=True)]
    all_gather x1 -> x0, waiting for transfers between devices: 49.6 us -> none  [local(): lax.all_gather(lax.all_to_all(dispatch, 'sp', split_axis=0, concat_axis=0...]
  transfers between devices with their start and end apart: 6 -> 5, of which waited for: 4 -> 3; matrix products, arithmetic and copies ran while one was open for 3% -> 2% of each run, Pallas kernels for 0% -> 0%
where the time goes in v1:
time: 367 us
  blocking collectives  205 us (56%)
  waiting for transfers between devices  81.9 us (22%)
  starting transfers between devices  22.4 us (6%)
  matrix products  22.2 us (6%)
  local copies, waits for them, and re-layouts  13.8 us (4%)
  between operations  13.7 us (4%)
  other arithmetic  7.69 us (2%)
    all_to_all x1, blocking collectives, local(): gathered_piece = lax.all_to_all(copies, 'tp', 0, 0, tiled=True)  187 us
    reduce_scatter x1, waiting for transfers between devices, local(): lax.psum_scatter(partial_value.astype(jnp.bfloat16), 'tp', scatter_dimens...  65.6 us
    all_to_all x1, blocking collectives, local(): lax.all_to_all(dispatch, 'sp', split_axis=0, concat_axis=0, tiled=True)  17.7 us
    dot_general x1, matrix products, local(): jnp.dot(activated, w_down[0], preferred_element_type=jnp.float32)  9.09 us
    all_to_all x1, starting transfers between devices, local(): lax.all_to_all(mixed_rows, 'tp', split_axis=0, concat_axis=1, tiled=True)  8.57 us
    all_to_all x1, waiting for transfers between devices, local(): lax.all_to_all(summed, 'sp', split_axis=0, concat_axis=0, tiled=True)  8.56 us
    all_to_all x1, waiting for transfers between devices, local(): lax.all_to_all(mixed_rows, 'tp', split_axis=0, concat_axis=1, tiled=True)  7.73 us
  transfers between devices with their start and end apart: 5, of which 3 were waited for; matrix products, arithmetic and copies ran while one was open for 2% of the time, Pallas kernels for 0%

profile of v1, /device:TPU:2, one launch (start us, length us, event | category | flops | bytes accessed | tf_op | source)
XLA Modules:
  0.0 366.6 jit_solution(16454332578900371784)
XLA Ops:
  6.5 0.0 copy-start
  6.5 0.9 slice.43
  7.4 3.4 collective-permute-start.1
  10.8 0.8 slice.38
  11.6 0.1 copy.45
  11.7 0.8 slice.39
  12.5 0.1 copy.46
  12.6 3.1 collective-permute-start
  15.7 0.9 convert_multiply_fusion
  16.6 0.7 convert_element_type.66
  17.3 0.7 convert_element_type.77
  18.0 0.8 copy.51
  18.8 0.1 reshape.83
  18.9 0.1 fusion.22
  18.9 0.1 reduce_window_sum.11
  19.0 0.2 select_reduce_fusion
  19.2 0.0 collective-permute-done.1
  19.2 0.8 pad_add_fusion
  20.0 0.8 fusion.24
  20.7 0.0 collective-permute-done
  20.8 0.1 copy.47
  20.9 1.0 fusion.19
  21.9 0.1 copy.48
  22.0 0.8 reshape.97
  22.8 8.6 %all-to-all-start = ((bf16[16,2,1024]{2,1,0:T(2,128)(2,1)}), bf16[16,2,1024]{2,1,0:T(2,128)(2,1)S(1)}, u32[]{:S(2)}, u32[]{:S(2)}) async-start(bf16[16,2,1024]{2,1,0:T(2,128)(2,1)} %reshape.97), calls=%async_computation | async-start | bytes 131072 | tf_op jit(solution)/shard_map/all_to_all | solution.py:50
  31.3 0.0 reduce-scatter.2.cloned.1.call-start
  31.4 7.7 %all-to-all-done = bf16[16,2,1024]{2,1,0:T(2,128)(2,1)S(1)} async-done(((bf16[16,2,1024]{2,1,0:T(2,128)(2,1)}), bf16[16,2,1024]{2,1,0:T(2,128)(2,1)S(1)}, u32[]{:S(2)}, u32[]{:S(2)}) %all-to-all-start) | async-done | bytes 65568 | tf_op jit(solution)/shard_map/all_to_all | solution.py:50
  39.1 0.1 reshape.98
  39.3 0.1 copy.49
  39.3 0.1 all_to_all.26
  39.5 3.1 multiply_reduce_fusion.1
  42.6 0.1 multiply_convert_fusion.1
  42.7 0.1 broadcast_in_dim.10
  42.9 0.1 reshape.84
  43.0 0.4 fusion.6
  43.4 17.7 %all_to_all.34 = bf16[16,8,2048]{2,1,0:T(8,128)(2,1)S(1)} all-to-all(bf16[16,8,2048]{2,1,0:T(8,128)(2,1)S(1)} %fusion.6), channel_id=1, replica_groups=mesh['sp'=16,'tp'=16] {'sp'}, dimensions={0} | all-to-all | bytes 1048576 | tf_op jit(solution)/shard_map/all_to_all | solution.py:73
  62.0 0.0 copy-start.3
  62.0 187.3 %all_to_all.35 = bf16[256,8,2048]{2,1,0:T(8,128)(2,1)S(1)} all-to-all(bf16[256,8,2048]{2,1,0:T(8,128)(2,1)S(1)} %constant_dynamic-update-slice_fusion), channel_id=1, replica_groups=mesh['sp'=16,'tp'=16] {'tp'}, dimensions={0} | all-to-all | bytes 16777216 | tf_op jit(solution)/shard_map/all_to_all | solution.py:75
  249.2 0.0 copy-done.3
  249.2 0.0 copy-start.4
  249.2 4.0 %fusion.2 = f32[2048,448]{0,1:T(8,128)S(1)} fusion(bf16[256,8,2048]{2,1,0:T(8,128)(2,1)S(1)} %all_to_all.35, bf16[1,2048,448]{1,2,0:T(8,128)(2,1)S(1)} %copy-done.3), kind=kOutput, calls=%fused_computation.3 | convolution fusion | flops 3758096384 | bytes 13893632 | tf_op jit(solution)/shard_map/dot_general | solution.py:77
  253.2 0.0 copy-done.4
  253.3 5.5 %multiply_convert_fusion = bf16[2048,448]{0,1:T(8,128)(2,1)} fusion(f32[2048,448]{0,1:T(8,128)S(1)} %fusion.2, bf16[256,8,2048]{2,1,0:T(8,128)(2,1)S(1)} %all_to_all.35, bf16[1,2048,448]{1,2,0:T(8,128)(2,1)S(1)} %copy-done.4), kind=kOutput, calls=%fused_computation.6 | convolution fusion | flops 3763601408 | bytes 15728640 | tf_op jit(solution)/shard_map/dot_general | solution.py:78
  258.8 3.8 %copy.54 = bf16[2048,448]{1,0:T(8,128)(2,1)} copy(bf16[2048,448]{0,1:T(8,128)(2,1)} %multiply_convert_fusion) | data formatting | bytes 3670016 | tf_op jit(solution)/shard_map/convert_element_type | solution.py:79
  262.6 0.0 copy-done
  262.6 9.1 %convolution_convert_fusion = bf16[256,8,2048]{2,0,1:T(8,128)(2,1)} fusion(bf16[256,8,448]{2,1,0:T(8,128)(2,1)} %bitcast.43, bf16[1,448,2048]{2,1,0:T(8,128)(2,1)S(1)} %copy-done), kind=kOutput, calls=%fused_computation.5 | convolution fusion | flops 3762290688 | bytes 12058624 | tf_op jit(solution)/shard_map/dot_general | solution.py:80
  271.7 0.0 copy-start.1
  271.7 0.0 reduce-scatter.2.cloned.1.call-update
  271.7 0.1 reduce_sum.32
  271.8 0.5 copy-done.1
  272.4 0.1 copy.57
  272.5 0.1 mul.151
  272.6 0.1 copy.52
  272.6 65.6 %reduce-scatter.2.cloned.1.call-done = bf16[16,8,2048]{2,0,1:T(8,128)(2,1)} async-done(((bf16[256,8,2048]{2,0,1:T(8,128)(2,1)}), bf16[16,8,2048]{2,0,1:T(8,128)(2,1)}) %reduce-scatter.2.cloned.1.call-update) | async-done | bytes 524304 | tf_op jit(solution)/shard_map/reduce_scatter | solution.py:84
  338.2 2.1 copy.56
  340.4 7.3 %all-to-all-start.3 = ((bf16[16,8,2048]{2,1,0:T(8,128)(2,1)}), bf16[16,8,2048]{2,1,0:T(8,128)(2,1)S(1)}, u32[]{:S(2)}, u32[]{:S(2)}) async-start(bf16[16,8,2048]{2,1,0:T(8,128)(2,1)} %copy.56), calls=%async_computation.4 | async-start | bytes 1048576 | tf_op jit(solution)/shard_map/all_to_all | solution.py:87
  347.6 0.1 copy.53
  347.7 0.0 copy-done.2
  347.8 0.1 copy.50
  347.9 8.6 %all-to-all-done.3 = bf16[16,8,2048]{2,1,0:T(8,128)(2,1)S(1)} async-done(((bf16[16,8,2048]{2,1,0:T(8,128)(2,1)}), bf16[16,8,2048]{2,1,0:T(8,128)(2,1)S(1)}, u32[]{:S(2)}, u32[]{:S(2)}) %all-to-all-start.3) | async-done | bytes 524320 | tf_op jit(solution)/shard_map/all_to_all | solution.py:87
  356.4 0.7 gather_fusion
  357.2 0.2 gather.7
  357.3 1.7 multiply_reduce_fusion
  359.1 0.7 add_convert_fusion
  (26 shorter events, 0.7 us)
Async XLA Ops:
  6.5 256.1 %copy-start = (bf16[1,448,2048]{2,1,0:T(8,128)(2,1)S(1)}, bf16[1,448,2048]{2,1,0:T(8,128)(2,1)}, u32[]{:S(2)}) copy-start(bf16[1,448,2048]{2,1,0:T(8,128)(2,1)} %param.25) | copy-start | bytes 5505028
  7.4 11.8 %collective-permute-start.1 = (s32[2]{0:T(128)S(1)}, s32[2]{0:T(128)S(1)}, u32[]{:S(2)}, u32[]{:S(2)}) collective-permute-start(s32[2]{0:T(128)S(1)} %slice.43), channel_id=1, source_target_pairs={{0,16},{16,32},{32,48},{48,64},{64,80},{80,96},{96,112},{112,128},... | collective-permute-start | bytes 32 | tf_op jit(solution)/shard_map/ppermute | solution.py:10
  12.6 8.1 %collective-permute-start = (bf16[2,2,64]{2,1,0:T(2,128)(2,1)S(1)}, bf16[2,2,64]{2,1,0:T(2,128)(2,1)S(1)}, u32[]{:S(2)}, u32[]{:S(2)}) collective-permute-start(bf16[2,2,64]{2,1,0:T(2,128)(2,1)S(1)} %pad_maximum_fusion.1), channel_id=1, source_target_pairs={{0,16},{16,32},{32,48},{48,64},{64,80},{80,96},{96,112},{112,128},... | collective-permute-start | bytes 1544 | tf_op jit(solution)/shard_map/ppermute | solution.py:10
  22.8 16.4 %all-to-all-start = ((bf16[16,2,1024]{2,1,0:T(2,128)(2,1)}), bf16[16,2,1024]{2,1,0:T(2,128)(2,1)S(1)}, u32[]{:S(2)}, u32[]{:S(2)}) async-start(bf16[16,2,1024]{2,1,0:T(2,128)(2,1)} %reshape.97), calls=%async_computation | async-start | bytes 131072 | tf_op jit(solution)/shard_map/all_to_all | solution.py:50
  31.3 306.9 %reduce-scatter.2.cloned.1.call-start = ((), (), s32[]{:S(2)}) async-start(), calls=%async_computation.5 | async-start | bytes 8912896 | tf_op jit(solution)/shard_map/reduce_scatter | solution.py:84
  62.0 187.3 %copy-start.3 = (bf16[1,2048,448]{1,2,0:T(8,128)(2,1)S(1)}, bf16[1,2048,448]{1,2,0:T(8,128)(2,1)}, u32[]{:S(2)}) copy-start(bf16[1,2048,448]{1,2,0:T(8,128)(2,1)} %param.23) | copy-start | bytes 5505028
  249.2 4.0 %copy-start.4 = (bf16[1,2048,448]{1,2,0:T(8,128)(2,1)S(1)}, bf16[1,2048,448]{1,2,0:T(8,128)(2,1)}, u32[]{:S(2)}) copy-start(bf16[1,2048,448]{1,2,0:T(8,128)(2,1)} %param.24) | copy-start | bytes 5505028
  271.7 0.7 copy-start.1
  271.7 76.1 %copy-start.2 = (f32[32,2]{0,1:T(2,128)S(1)}, f32[32,2]{0,1:T(2,128)}, u32[]{:S(2)}) copy-start(f32[32,2]{0,1:T(2,128)} %param.22) | copy-start | bytes 772
  340.4 16.1 %all-to-all-start.3 = ((bf16[16,8,2048]{2,1,0:T(8,128)(2,1)}), bf16[16,8,2048]{2,1,0:T(8,128)(2,1)S(1)}, u32[]{:S(2)}, u32[]{:S(2)}) async-start(bf16[16,8,2048]{2,1,0:T(8,128)(2,1)} %copy.56), calls=%async_computation.4 | async-start | bytes 1048576 | tf_op jit(solution)/shard_map/all_to_all | solution.py:87
Sparse Core Ops, SparseCore 0:
  271.8 66.3 reduce-scatter.1
